TPU v7x, 32 devices: a whole 2x2x4 slice. The times are simulated.
32 devices in a mesh: grp: 2 (over y), sp: 4 (over z), tp: 4 (over x, core).
Axes of the slice: x: 2, y: 2, z: 4, core: 2. Of those that a mesh axis runs over, the one named last changes fastest.
Arguments:
- tokens: bfloat16 [3072, 4096], P(('grp', 'sp'), 'tp'), parts along dimension 0, may hold values from -6 to 6
- proj_b: bfloat16 [2, 4096, 2048], P(None, 'sp', 'tp'), may hold values from -0.09375 to 0.09375
- proj_c: bfloat16 [2, 4096, 2048], P(None, 'sp', 'tp'), may hold values from -0.09375 to 0.09375
- proj_x: bfloat16 [2, 4096, 2048], P(None, 'sp', 'tp'), may hold values from -0.09375 to 0.09375
- proj_out: bfloat16 [2, 2048, 4096], P(None, 'sp', 'tp'), may hold values from -1 to 1
- conv_taps: float32 [2, 3, 2048], P(None, None, 'tp'), may hold values from -3 to 3
- ln_gain: float32 [2, 4096], P(None, 'tp'), may hold values from 0.1 to 1.9
- ln_bias: float32 [2, 4096], P(None, 'tp'), may hold values from -2 to 2
Outputs:
- result: bfloat16 [3072, 4096], P(('grp', 'sp'), 'tp'), parts along dimension 0
There are 2 independent parts, one for each index of `grp`. A program takes and returns all parts, laid end to end along the dimension named above; an argument that names none is the same for every part. Nothing has to cross between parts.
All inputs are finite; a program needn't handle non-finite values.
Results may differ from a plain program's by a relative error of at most 0.012.
Values may be sent and summed in bfloat16 or wider, within the bound.
A program may use at most 128 MiB of HBM per device.

v0:
```python
import jax
import jax.numpy as jnp
from jax import lax
from jax.sharding import PartitionSpec as P

LAYERS = 2


norm_eps = 1e-05


def from_behind(block, axis, distance):
    devices = range(lax.axis_size(axis))
    route = [(i - distance, i) for i in devices if i - distance in devices]
    return lax.ppermute(block, axis, route)


def local(tokens, proj_b, proj_c, proj_x, proj_out, conv_taps, ln_gain, ln_bias):
    residual_scale = (2.0 * LAYERS) ** 0.25
    hidden = tokens
    whole_b, whole_c, whole_x, whole_out = (
        lax.all_gather(proj_b, "sp", axis=1, tiled=True),
        lax.all_gather(proj_c, "sp", axis=1, tiled=True),
        lax.all_gather(proj_x, "sp", axis=1, tiled=True),
        lax.all_gather(proj_out, "sp", axis=1, tiled=True),
    )
    for layer_index in range(LAYERS):
        gathered = lax.all_gather(hidden, "tp", axis=1, tiled=True)
        count_rows = gathered.shape[0]
        acc_b = jnp.dot(gathered, whole_b[layer_index], preferred_element_type=jnp.float32)
        acc_c = jnp.dot(gathered, whole_c[layer_index], preferred_element_type=jnp.float32)
        acc_x = jnp.dot(gathered, whole_x[layer_index], preferred_element_type=jnp.float32)
        out_gate = lax.optimization_barrier(acc_b.astype(jnp.bfloat16))
        in_gate = lax.optimization_barrier(acc_c.astype(jnp.bfloat16))
        values = lax.optimization_barrier(acc_x.astype(jnp.bfloat16))
        gated_in = in_gate.astype(jnp.float32) * values.astype(jnp.float32)
        reach = conv_taps.shape[1] - 1
        fringe = from_behind(gated_in[count_rows - reach :], "sp", 1)
        padded = jnp.concatenate([fringe, gated_in], 0)
        conv_out = jnp.zeros_like(gated_in)
        for tap_index in range(reach + 1):
            conv_out = (
                conv_out
                + conv_taps[layer_index, tap_index] * padded[tap_index : tap_index + count_rows]
            )
        branch = (out_gate.astype(jnp.float32) * conv_out).astype(jnp.bfloat16)
        all_branch = lax.all_gather(branch, "tp", axis=1, tiled=True)
        acc_out = jnp.dot(all_branch, whole_out[layer_index], preferred_element_type=jnp.float32)
        mixed = lax.optimization_barrier(acc_out.astype(jnp.bfloat16))
        summed = residual_scale * hidden.astype(jnp.float32) + mixed.astype(jnp.float32)
        width_all = summed.shape[1] * lax.axis_size("tp")
        mean = (lax.psum(jnp.sum(summed, axis=1), "tp") / width_all)[:, None]
        centered = summed - mean
        variance = (lax.psum(jnp.sum(centered * centered, axis=1), "tp") / width_all)[:, None]
        hidden = (
            centered * lax.rsqrt(variance + norm_eps) * ln_gain[layer_index] + ln_bias[layer_index]
        ).astype(jnp.bfloat16)
    return hidden


def solution(mesh):
    return jax.shard_map(
        local,
        mesh=mesh,
        in_specs=(
            P(("grp", "sp"), "tp"),
            P(None, "sp", "tp"),
            P(None, "sp", "tp"),
            P(None, "sp", "tp"),
            P(None, "sp", "tp"),
            P(None, None, "tp"),
            P(None, "tp"),
            P(None, "tp"),
        ),
        out_specs=P(("grp", "sp"), "tp"),
        check_vma=False,
    )
```

profile of v0, /device:TPU:0, one launch (start us, length us, event | category | flops | bytes accessed | tf_op | source)
XLA Modules:
  0.0 767.4 jit_solution(15799623841625418125)
XLA Ops:
  6.5 0.7 all-gather.9.cloned.1.call-update
  7.3 0.0 all-gather.13.cloned.1.call-start
  7.3 0.7 all-gather.13.cloned.1.call-update
  8.0 0.0 all-gather.15.cloned.1.call-start
  8.1 0.7 all-gather.15.cloned.1.call-update
  8.8 0.0 all-gather.11.cloned.1.call-start
  8.8 0.5 all-gather.11.cloned.1.call-update
  9.3 0.0 all-gather.19.cloned.1.call-start
  9.4 0.5 all-gather.19.cloned.1.call-update
  9.9 0.0 all-gather.17.cloned.1.call-start
  10.0 30.2 %all-gather.9.cloned.1.call-done = bf16[384,4096]{1,0:T(8,128)(2,1)} async-done(((bf16[384,1024]{1,0:T(8,128)(2,1)}), bf16[384,4096]{1,0:T(8,128)(2,1)}) %all-gather.9.cloned.1.call-update) | async-done | bytes 3145744 | tf_op jit(solution)/shard_map/all_gather | solution.py:28
  40.2 151.2 %all-gather.13.cloned.1.call-done = bf16[2,4096,512]{2,1,0:T(8,128)(2,1)} async-done(((bf16[2,1024,512]{2,1,0:T(8,128)(2,1)}), bf16[2,4096,512]{2,1,0:T(8,128)(2,1)}) %all-gather.13.cloned.1.call-update) | async-done | bytes 8388624 | tf_op jit(solution)/shard_map/all_gather | solution.py:23
  191.4 4.9 fusion.11
  196.3 144.5 %all-gather.15.cloned.1.call-done = bf16[2,4096,512]{2,1,0:T(8,128)(2,1)} async-done(((bf16[2,1024,512]{2,1,0:T(8,128)(2,1)}), bf16[2,4096,512]{2,1,0:T(8,128)(2,1)}) %all-gather.15.cloned.1.call-update) | async-done | bytes 8388624 | tf_op jit(solution)/shard_map/all_gather | solution.py:24
  340.8 4.9 fusion.12
  345.7 0.1 convert_multiply_fusion.1
  345.8 1.3 collective-permute-start
  347.1 142.9 %all-gather.11.cloned.1.call-done = bf16[2,4096,512]{2,1,0:T(8,128)(2,1)} async-done(((bf16[2,1024,512]{2,1,0:T(8,128)(2,1)}), bf16[2,4096,512]{2,1,0:T(8,128)(2,1)}) %all-gather.11.cloned.1.call-update) | async-done | bytes 8388624 | tf_op jit(solution)/shard_map/all_gather | solution.py:22
  490.0 4.9 fusion.10
  495.0 0.0 copy-start.3
  495.0 1.1 fusion.29
  496.1 0.0 all-gather.17.cloned.1.call-update
  496.1 0.0 all-gather.21.cloned.1.call-start
  496.2 143.1 %all-gather.19.cloned.1.call-done = bf16[2,2048,1024]{2,1,0:T(8,128)(2,1)} async-done(((bf16[2,512,1024]{2,1,0:T(8,128)(2,1)}), bf16[2,2048,1024]{2,1,0:T(8,128)(2,1)}) %all-gather.19.cloned.1.call-update) | async-done | bytes 8388624 | tf_op jit(solution)/shard_map/all_gather | solution.py:25
  639.3 19.3 %all-gather.17.cloned.1.call-done = bf16[384,2048]{1,0:T(8,128)(2,1)} async-done(((bf16[384,512]{1,0:T(8,128)(2,1)}), bf16[384,2048]{1,0:T(8,128)(2,1)}) %all-gather.17.cloned.1.call-update) | async-done | bytes 1572880 | tf_op jit(solution)/shard_map/all_gather | solution.py:47
  658.6 4.5 fusion.8
  663.0 0.3 fusion.16
  663.4 5.9 psum.28
  669.2 0.4 multiply_reduce_fusion.1
  669.7 5.7 psum.29
  675.3 1.3 add_convert_fusion.1
  676.7 0.0 all-gather.21.cloned.1.call-update
  676.7 0.0 all-gather.23.cloned.1.call-start
  676.8 29.9 %all-gather.21.cloned.1.call-done = bf16[384,4096]{1,0:T(8,128)(2,1)} async-done(((bf16[384,1024]{1,0:T(8,128)(2,1)}), bf16[384,4096]{1,0:T(8,128)(2,1)}) %all-gather.21.cloned.1.call-update) | async-done | bytes 3145744 | tf_op jit(solution)/shard_map/all_gather | solution.py:28
  706.7 5.1 fusion.14
  711.8 4.1 fusion.15
  715.9 0.1 convert_multiply_fusion
  716.0 3.6 collective-permute-start.1
  719.6 1.8 fusion.13
  721.4 1.0 fusion.23
  722.5 0.0 all-gather.23.cloned.1.call-update
  722.5 19.9 %all-gather.23.cloned.1.call-done = bf16[384,2048]{1,0:T(8,128)(2,1)} async-done(((bf16[384,512]{1,0:T(8,128)(2,1)}), bf16[384,2048]{1,0:T(8,128)(2,1)}) %all-gather.23.cloned.1.call-update) | async-done | bytes 1572880 | tf_op jit(solution)/shard_map/all_gather | solution.py:47
  742.4 4.5 fusion.9
  746.9 0.3 fusion.17
  747.2 5.9 psum.30
  753.1 0.4 multiply_reduce_fusion
  753.5 5.7 psum.31
  759.2 1.3 add_convert_fusion
  (28 shorter events, 0.1 us)
Async XLA Ops:
  6.5 33.6 %all-gather.9.cloned.1.call-start = ((), (), s32[]{:S(2)}) async-start(), calls=%async_computation | async-start | bytes 3932160 | tf_op jit(solution)/shard_map/all_gather | solution.py:28
  7.3 184.1 %all-gather.13.cloned.1.call-start = ((), (), s32[]{:S(2)}) async-start(), calls=%async_computation.2 | async-start | bytes 10485760 | tf_op jit(solution)/shard_map/all_gather | solution.py:23
  8.0 332.8 %all-gather.15.cloned.1.call-start = ((), (), s32[]{:S(2)}) async-start(), calls=%async_computation.3 | async-start | bytes 10485760 | tf_op jit(solution)/shard_map/all_gather | solution.py:24
  8.7 1.2 copy-start.2
  8.8 481.3 %all-gather.11.cloned.1.call-start = ((), (), s32[]{:S(2)}) async-start(), calls=%async_computation.1 | async-start | bytes 10485760 | tf_op jit(solution)/shard_map/all_gather | solution.py:22
  9.3 630.0 %all-gather.19.cloned.1.call-start = ((), (), s32[]{:S(2)}) async-start(), calls=%async_computation.5 | async-start | bytes 10485760 | tf_op jit(solution)/shard_map/all_gather | solution.py:25
  9.9 648.6 %all-gather.17.cloned.1.call-start = ((), (), s32[]{:S(2)}) async-start(), calls=%async_computation.4 | async-start | bytes 1966080 | tf_op jit(solution)/shard_map/all_gather | solution.py:47
  345.8 149.2 %collective-permute-start = (f32[2,512]{1,0:T(2,128)S(1)}, f32[2,512]{1,0:T(2,128)S(1)}, u32[]{:S(2)}, u32[]{:S(2)}) collective-permute-start(f32[2,512]{1,0:T(2,128)S(1)} %slice.99), channel_id=1, source_target_pairs={{0,4},{4,8},{8,12},{1,5},{5,9},{9,13},{2,6},{6,10},{10,14},{3,7},{... | collective-permute-start | bytes 12296 | tf_op jit(solution)/shard_map/ppermute | solution.py:15
  495.0 1.2 copy-start.3
  495.0 1.2 copy-start.4
  496.1 210.6 %all-gather.21.cloned.1.call-start = ((), (), s32[]{:S(2)}) async-start(), calls=%async_computation.6 | async-start | bytes 3932160 | tf_op jit(solution)/shard_map/all_gather | solution.py:28
  496.2 166.8 %copy-start.1 = (bf16[384,1024]{1,0:T(8,128)(2,1)S(1)}, bf16[384,1024]{1,0:T(8,128)(2,1)}, u32[]{:S(2)}) copy-start(bf16[384,1024]{1,0:T(8,128)(2,1)} %param.8) | copy-start | bytes 2359300
  676.7 65.7 %all-gather.23.cloned.1.call-start = ((), (), s32[]{:S(2)}) async-start(), calls=%async_computation.7 | async-start | bytes 1966080 | tf_op jit(solution)/shard_map/all_gather | solution.py:47
  706.7 5.1 copy-start.5
  706.7 12.9 %slice-start = ((s8[8388608]{0:T(1024)(128)(4,1)}), s8[4194304]{0:T(1024)(128)(4,1)S(1)}, s32[]{:S(2)}) async-start(s8[8388608]{0:T(1024)(128)(4,1)} %bitcast.68), calls=%async_computation.8 | async-start | bytes 8388608
  711.8 7.9 %slice-start.1 = ((s8[8388608]{0:T(1024)(128)(4,1)}), s8[4194304]{0:T(1024)(128)(4,1)S(1)}, s32[]{:S(2)}) async-start(s8[8388608]{0:T(1024)(128)(4,1)} %bitcast.68), calls=%async_computation.9 | async-start | bytes 8388608
  716.0 5.4 collective-permute-start.1
  722.5 24.3 %copy-start = (bf16[384,1024]{1,0:T(8,128)(2,1)S(1)}, bf16[384,1024]{1,0:T(8,128)(2,1)}, u32[]{:S(2)}) copy-start(bf16[384,1024]{1,0:T(8,128)(2,1)} %add_convert_fusion.1) | copy-start | bytes 2359300
Sparse Core Ops, SparseCore 0:
  8.9 31.2 all-gather.8
  41.7 149.6 all-gather.12
  192.9 147.7 all-gather.14
  342.2 147.7 all-gather.10
  491.5 147.7 all-gather.18
  640.7 17.8 all-gather.16
  676.8 29.8 all-gather.20
  722.6 19.7 all-gather.22
where the time goes:
time: 768 us; the launch traced here: 767 us
  waiting for transfers between devices  684 us (89%)
  matrix products  34.6 us (5%)
  blocking collectives  23.1 us (3%)
  between operations  13.8 us (2%)
    all_gather x1, waiting for transfers between devices, local(): lax.all_gather(proj_c, 'sp', axis=1, tiled=True)  151 us
    all_gather x1, waiting for transfers between devices, local(): lax.all_gather(proj_x, 'sp', axis=1, tiled=True)  144 us
    all_gather x1, waiting for transfers between devices, local(): lax.all_gather(proj_out, 'sp', axis=1, tiled=True)  143 us
    all_gather x1, waiting for transfers between devices, local(): lax.all_gather(proj_b, 'sp', axis=1, tiled=True)  143 us
    all_gather x2, waiting for transfers between devices, local(): gathered = lax.all_gather(hidden, 'tp', axis=1, tiled=True)  60.1 us
    all_gather x2, waiting for transfers between devices, local(): all_branch = lax.all_gather(branch, 'tp', axis=1, tiled=True)  39.1 us
  transfers between devices with their start and end apart: 10, of which 8 were waited for; matrix products, arithmetic and copies ran while one was open for 2% of the time, Pallas kernels for 0%

commit v1 on v0

v1 whole, which is shorter than its diff:
```python
import jax
import jax.numpy as jnp
from jax import lax
from jax.sharding import PartitionSpec as P

LAYERS = 2


norm_eps = 1e-05


def from_behind(block, axis, distance):
    devices = range(lax.axis_size(axis))
    route = [(i - distance, i) for i in devices if i - distance in devices]
    return lax.ppermute(block, axis, route)


def local(tokens, proj_b, proj_c, proj_x, proj_out, conv_taps, ln_gain, ln_bias):
    residual_scale = (2.0 * LAYERS) ** 0.25
    parts = lax.axis_size("grp")
    me = lax.axis_index("grp")
    rows = tokens.shape[0]
    wide = proj_b.shape[2] // parts
    out_wide = proj_out.shape[2] // parts

    def mine(array, width):
        return lax.dynamic_slice_in_dim(array, me * width, width, array.ndim - 1)

    weights = []
    for layer_index in range(LAYERS):
        ins = jnp.concatenate(
            [mine(w[layer_index], wide) for w in (proj_b, proj_c, proj_x)], axis=1
        )
        weights.append(
            (
                lax.all_gather(ins, "sp", axis=0, tiled=True),
                lax.all_gather(mine(proj_out[layer_index], out_wide), "sp", axis=0, tiled=True),
            )
        )
    taps, gain, bias = mine(conv_taps, wide), mine(ln_gain, out_wide), mine(ln_bias, out_wide)
    swapped = lax.all_to_all(
        tokens.reshape(rows, parts, out_wide), "grp", split_axis=1, concat_axis=0, tiled=False
    )
    hidden = swapped.reshape(parts * rows, out_wide)
    reach = taps.shape[1] - 1
    for layer_index in range(LAYERS):
        whole_in, whole_out = weights[layer_index]
        gathered = lax.all_gather(hidden, ("tp", "grp"), axis=1, tiled=True)
        acc = jnp.dot(gathered, whole_in, preferred_element_type=jnp.float32)
        acc = lax.optimization_barrier(acc.astype(jnp.bfloat16)).astype(jnp.float32)
        out_gate, in_gate, values = (acc[:, i * wide : (i + 1) * wide] for i in range(3))
        gated_in = (in_gate * values).reshape(parts, rows, wide)
        fringe = from_behind(gated_in[:, rows - reach :], "sp", 1)
        padded = jnp.concatenate([fringe, gated_in], 1)
        conv_out = jnp.zeros_like(gated_in)
        for tap_index in range(reach + 1):
            conv_out = (
                conv_out + taps[layer_index, tap_index] * padded[:, tap_index : tap_index + rows]
            )
        branch = (out_gate * conv_out.reshape(parts * rows, wide)).astype(jnp.bfloat16)
        all_branch = lax.all_gather(branch, ("tp", "grp"), axis=1, tiled=True)
        acc_out = jnp.dot(all_branch, whole_out, preferred_element_type=jnp.float32)
        mixed = lax.optimization_barrier(acc_out.astype(jnp.bfloat16))
        summed = residual_scale * hidden.astype(jnp.float32) + mixed.astype(jnp.float32)
        width_all = summed.shape[1] * lax.axis_size(("tp", "grp"))
        mean = (lax.psum(jnp.sum(summed, axis=1), ("tp", "grp")) / width_all)[:, None]
        centered = summed - mean
        variance = (lax.psum(jnp.sum(centered * centered, axis=1), ("tp", "grp")) / width_all)[
            :, None
        ]
        hidden = (
            centered * lax.rsqrt(variance + norm_eps) * gain[layer_index] + bias[layer_index]
        ).astype(jnp.bfloat16)
    back = lax.all_to_all(
        hidden.reshape(parts, rows, out_wide), "grp", split_axis=0, concat_axis=1, tiled=False
    )
    return back.reshape(rows, parts * out_wide)


def solution(mesh):
    return jax.shard_map(
        local,
        mesh=mesh,
        in_specs=(
            P(("grp", "sp"), "tp"),
            P(None, "sp", "tp"),
            P(None, "sp", "tp"),
            P(None, "sp", "tp"),
            P(None, "sp", "tp"),
            P(None, None, "tp"),
            P(None, "tp"),
            P(None, "tp"),
        ),
        out_specs=P(("grp", "sp"), "tp"),
        check_vma=False,
    )
```

time: 768 us -> 563 us (0.73)
  waiting for transfers between devices: 684 us -> 402 us
  blocking collectives: 23.1 us -> 82.4 us
  local copies, waits for them, and re-layouts: 0.08 us -> 17.8 us
  matrix products: 34.6 us -> 26.7 us
    all_gather x8, waiting for transfers between devices: 681 us -> 388 us  [the longest x2 179 us: local(): lax.all_gather(ins, 'sp', axis=0, tiled=True)]
    psum x4, blocking collectives: 23.1 us -> 53.1 us  [the longest x2 26.7 us: local(): lax.psum(jnp.sum(centered * centered, axis=1), ('tp', 'grp')) / width_all]
    all_to_all x0 -> x2, blocking collectives: none -> 29.2 us  [the longest x1 15.5 us: local(): lax.all_to_all(tokens.reshape(rows, parts, out_wide), 'grp', split_axis=1...]
    ppermute x2, waiting for transfers between devices: 0.01 us -> 13.3 us  [from_behind(): return lax.ppermute(block, axis, route)]
    slice x5 -> x8, local copies, waits for them, and re-layouts: 0.04 us -> 8.24 us  [the longest x3 5.03 us: local(): w[layer_index]]
    dot_general x8 -> x4, matrix products: 34.6 us -> 26.7 us  [the longest x2 18.1 us: local(): acc = jnp.dot(gathered, whole_in, preferred_element_type=jnp.float32)]
  transfers between devices with their start and end apart: 10 -> 10, of which waited for: 8 -> 10; matrix products, arithmetic and copies ran while one was open for 2% -> 7% of each run, Pallas kernels for 0% -> 0%
where the time goes in v1:
time: 563 us; the launch traced here: 562 us
  waiting for transfers between devices  402 us (71%)
  blocking collectives  82.4 us (15%)
  matrix products  26.7 us (5%)
  local copies, waits for them, and re-layouts  17.8 us (3%)
  between operations  13.7 us (2%)
  other arithmetic  12.4 us (2%)
  starting transfers between devices  7.33 us (1%)
    all_gather x2, waiting for transfers between devices, local(): lax.all_gather(ins, 'sp', axis=0, tiled=True)  179 us
    all_gather x2, waiting for transfers between devices, local(): gathered = lax.all_gather(hidden, ('tp', 'grp'), axis=1, tiled=True)  93.2 us
    all_gather x2, waiting for transfers between devices, local(): all_branch = lax.all_gather(branch, ('tp', 'grp'), axis=1, tiled=True)  69.4 us
    all_gather x2, waiting for transfers between devices, local(): lax.all_gather(mine(proj_out[layer_index], out_wide), 'sp', axis=0, tiled...  46.5 us
    psum x2, blocking collectives, local(): lax.psum(jnp.sum(centered * centered, axis=1), ('tp', 'grp')) / width_all  26.7 us
    psum x2, blocking collectives, local(): lax.psum(jnp.sum(summed, axis=1), ('tp', 'grp')) / width_all  26.4 us
    dot_general x2, matrix products, local(): acc = jnp.dot(gathered, whole_in, preferred_element_type=jnp.float32)  18.1 us
    all_to_all x1, blocking collectives, local(): lax.all_to_all(tokens.reshape(rows, parts, out_wide), 'grp', split_axis=1...  15.5 us
  transfers between devices with their start and end apart: 10, of which 10 were waited for; matrix products, arithmetic and copies ran while one was open for 7% of the time, Pallas kernels for 0%

profile of v1, /device:TPU:0, one launch (start us, length us, event | category | flops | bytes accessed | tf_op | source)
XLA Modules:
  0.0 562.1 jit_solution(15424829978587201237)
XLA Ops:
  6.5 2.8 fusion.27
  9.3 1.1 fusion.28
  10.5 0.8 copy-done.6
  11.3 1.1 fusion.26
  12.5 1.3 pad_maximum_fusion
  13.9 1.1 copy-done.7
  14.9 0.4 copy.12
  15.6 15.5 %all_to_all.30 = bf16[1,384,2,512]{3,1,0,2:T(8,128)(2,1)} all-to-all(bf16[1,384,2,512]{3,1,0,2:T(8,128)(2,1)S(1)} %copy.13), channel_id=1, replica_groups=mesh['grp'=2,'sp'=4,'tp'=4] {'grp'}, dimensions={2} | all-to-all | bytes 1572864 | tf_op jit(solution)/shard_map/all_to_all | solution.py:41
  31.2 2.7 fusion.25
  33.9 0.8 constant_dynamic-slice_fusion.6
  34.8 97.2 %all-gather.11.cloned.1.call-done = bf16[4096,768]{1,0:T(8,128)(2,1)} async-done(((bf16[1024,768]{1,0:T(8,128)(2,1)}), bf16[4096,768]{1,0:T(8,128)(2,1)}) %all-gather.11.cloned.1.call-update) | async-done | bytes 6291472 | tf_op jit(solution)/shard_map/all_gather | solution.py:36
  132.0 46.7 %all-gather.13.cloned.1.call-done = bf16[768,4096]{1,0:T(8,128)(2,1)} async-done(((bf16[768,512]{1,0:T(8,128)(2,1)}), bf16[768,4096]{1,0:T(8,128)(2,1)}) %all-gather.13.cloned.1.call-update) | async-done | bytes 6291472 | tf_op jit(solution)/shard_map/all_gather | solution.py:48
  178.7 9.1 %fusion.10 = bf16[768,768]{0,1:T(8,128)(2,1)S(1)} fusion(bf16[4096,768]{1,0:T(8,128)(2,1)} %all-gather.11.cloned.1.call-done, bf16[768,4096]{1,0:T(8,128)(2,1)} %all-gather.13.cloned.1.call-done), kind=kOutput, calls=%fused_computation.16 | convolution fusion | flops 4832428032 | bytes 13762560 | tf_op jit(solution)/shard_map/dot_general | solution.py:49
  188.0 1.0 slice_multiply_fusion.2
  188.9 1.6 reshape.30
  190.5 0.3 slice.123
  190.8 3.5 collective-permute-start
  194.4 12.0 %collective-permute-done = f32[2,2,256]{1,0,2:T(2,128)S(1)} collective-permute-done((f32[2,2,256]{1,0,2:T(2,128)S(1)}, f32[2,2,256]{1,0,2:T(2,128)S(1)}, u32[]{:S(2)}, u32[]{:S(2)}) %collective-permute-start) | collective-permute-done | bytes 4128 | tf_op jit(solution)/shard_map/ppermute | solution.py:15
  206.4 3.1 fusion.20
  209.6 0.8 fusion.24
  210.5 1.2 dynamic-slice_bitcast_fusion.2
  212.0 1.3 pad_maximum_fusion.1
  213.3 0.6 copy-done.9
  214.0 14.3 %all-gather.23.cloned.1.call-done = bf16[1,2048,512]{2,1,0:T(8,128)(2,1)} async-done(((bf16[1,512,512]{2,1,0:T(8,128)(2,1)}), bf16[1,2048,512]{2,1,0:T(8,128)(2,1)}) %all-gather.23.cloned.1.call-update) | async-done | bytes 2097168 | tf_op jit(solution)/shard_map/all_gather | solution.py:37
  228.3 35.9 %all-gather.15.cloned.1.call-done = bf16[768,2048]{0,1:T(8,128)(2,1)} async-done(((bf16[768,256]{0,1:T(8,128)(2,1)}), bf16[768,2048]{0,1:T(8,128)(2,1)}) %all-gather.15.cloned.1.call-update) | async-done | bytes 3145744 | tf_op jit(solution)/shard_map/all_gather | solution.py:61
  264.3 4.4 fusion.4
  268.6 0.3 fusion.11
  269.0 13.3 %psum.28 = f32[768]{0:T(1024)S(1)} all-reduce(f32[768]{0:T(1024)S(1)} %fusion.11), channel_id=1, replica_groups=mesh['grp'=2,'sp'=4,'tp'=4] {'tp','grp'}, use_global_device_ids=true, to_apply=%region_1.0 | all-reduce | flops 768 | bytes 6144 | tf_op jit(solution)/shard_map/psum | solution.py:66
  282.2 0.5 multiply_reduce_fusion.1
  282.7 13.7 %psum.29 = f32[768]{0:T(1024)S(1)} all-reduce(f32[768]{0:T(1024)S(1)} %multiply_reduce_fusion.1), channel_id=1, replica_groups=mesh['grp'=2,'sp'=4,'tp'=4] {'tp','grp'}, use_global_device_ids=true, to_apply=%region_3.0 | all-reduce | flops 768 | bytes 6144 | tf_op jit(solution)/shard_map/psum | solution.py:68
  296.5 1.4 add_convert_fusion.1
  297.9 0.8 constant_dynamic-slice_fusion.3
  299.0 82.1 %all-gather.19.cloned.1.call-done = bf16[4096,768]{1,0:T(8,128)(2,1)} async-done(((bf16[1024,768]{1,0:T(8,128)(2,1)}), bf16[4096,768]{1,0:T(8,128)(2,1)}) %all-gather.19.cloned.1.call-update) | async-done | bytes 6291472 | tf_op jit(solution)/shard_map/all_gather | solution.py:36
  381.0 46.5 %all-gather.17.cloned.1.call-done = bf16[768,4096]{1,0:T(8,128)(2,1)} async-done(((bf16[768,512]{1,0:T(8,128)(2,1)}), bf16[768,4096]{1,0:T(8,128)(2,1)}) %all-gather.17.cloned.1.call-update) | async-done | bytes 6291472 | tf_op jit(solution)/shard_map/all_gather | solution.py:48
  427.6 9.0 %convolution_convert_fusion = bf16[768,768]{1,0:T(8,128)(2,1)S(1)} fusion(bf16[768,4096]{1,0:T(8,128)(2,1)} %all-gather.17.cloned.1.call-done, bf16[4096,768]{1,0:T(8,128)(2,1)} %all-gather.19.cloned.1.call-done), kind=kOutput, calls=%fused_computation.12 | convolution fusion | flops 4832428032 | bytes 13762560 | tf_op jit(solution)/shard_map/dot_general | solution.py:49
  436.8 3.4 collective-permute-start.1
  440.2 1.3 collective-permute-done.1
  441.8 0.9 fusion.22
  442.7 32.1 %all-gather.25.cloned.1.call-done = bf16[1,2048,512]{2,1,0:T(8,128)(2,1)} async-done(((bf16[1,512,512]{2,1,0:T(8,128)(2,1)}), bf16[1,2048,512]{2,1,0:T(8,128)(2,1)}) %all-gather.25.cloned.1.call-update) | async-done | bytes 2097168 | tf_op jit(solution)/shard_map/all_gather | solution.py:37
  474.8 33.5 %all-gather.21.cloned.1.call-done = bf16[768,2048]{1,0:T(8,128)(2,1)} async-done(((bf16[768,256]{1,0:T(8,128)(2,1)}), bf16[768,2048]{1,0:T(8,128)(2,1)}) %all-gather.21.cloned.1.call-update) | async-done | bytes 3145744 | tf_op jit(solution)/shard_map/all_gather | solution.py:61
  508.3 4.3 fusion.7
  512.9 13.2 %psum.30 = f32[768]{0:T(1024)S(1)} all-reduce(f32[768]{0:T(1024)S(1)} %fusion.12), channel_id=1, replica_groups=mesh['grp'=2,'sp'=4,'tp'=4] {'tp','grp'}, use_global_device_ids=true, to_apply=%region_5.0 | all-reduce | flops 768 | bytes 6144 | tf_op jit(solution)/shard_map/psum | solution.py:66
  526.1 0.5 multiply_reduce_fusion
  526.6 13.0 %psum.31 = f32[768]{0:T(1024)S(1)} all-reduce(f32[768]{0:T(1024)S(1)} %multiply_reduce_fusion), channel_id=1, replica_groups=mesh['grp'=2,'sp'=4,'tp'=4] {'tp','grp'}, use_global_device_ids=true, to_apply=%region_7.0 | all-reduce | flops 768 | bytes 6144 | tf_op jit(solution)/shard_map/psum | solution.py:68
  539.6 0.5 add_convert_fusion
  540.0 13.7 %all_to_all.31 = bf16[2,384,1,512]{3,1,2,0:T(8,128)(2,1)S(1)} all-to-all(bf16[2,384,1,512]{3,1,2,0:T(8,128)(2,1)S(1)} %bitcast.71), channel_id=1, replica_groups=mesh['grp'=2,'sp'=4,'tp'=4] {'grp'}, dimensions={0} | all-to-all | bytes 1572864 | tf_op jit(solution)/shard_map/all_to_all | solution.py:74
  553.7 0.4 copy.15
  554.1 1.2 copy.16
  (52 shorter events, 2.6 us)
Async XLA Ops:
  6.5 125.5 %all-gather.11.cloned.1.call-start = ((), (), s32[]{:S(2)}) async-start(), calls=%async_computation.2 | async-start | bytes 7864320 | tf_op jit(solution)/shard_map/all_gather | solution.py:36
  6.5 2.8 copy-start.5
  9.3 2.0 copy-start.6
  13.8 1.1 copy-start.7
  13.8 164.9 %all-gather.13.cloned.1.call-start = ((), (), s32[]{:S(2)}) async-start(), calls=%async_computation.3 | async-start | bytes 7077888 | tf_op jit(solution)/shard_map/all_gather | solution.py:48
  31.1 197.2 %all-gather.23.cloned.1.call-start = ((), (), s32[]{:S(2)}) async-start(), calls=%async_computation.8 | async-start | bytes 2621440 | tf_op jit(solution)/shard_map/all_gather | solution.py:37
  34.7 229.5 %all-gather.15.cloned.1.call-start = ((), (), s32[]{:S(2)}) async-start(), calls=%async_computation.4 | async-start | bytes 3538944 | tf_op jit(solution)/shard_map/all_gather | solution.py:61
  188.9 5.4 copy-start.8
  190.8 15.5 %collective-permute-start = (f32[2,2,256]{1,0,2:T(2,128)S(1)}, f32[2,2,256]{1,0,2:T(2,128)S(1)}, u32[]{:S(2)}, u32[]{:S(2)}) collective-permute-start(f32[2,2,256]{1,0,2:T(2,128)S(1)} %slice.123), channel_id=1, source_target_pairs={{0,4},{4,8},{8,12},{1,5},{5,9},{9,13},{2,6},{6,10},{10,14},{3,7},{... | collective-permute-start | bytes 12296 | tf_op jit(solution)/shard_map/ppermute | solution.py:15
  209.6 2.1 copy-start.2
  210.4 1.5 copy-start.3
  210.4 170.6 %all-gather.19.cloned.1.call-start = ((), (), s32[]{:S(2)}) async-start(), calls=%async_computation.6 | async-start | bytes 7864320 | tf_op jit(solution)/shard_map/all_gather | solution.py:36
  213.2 0.7 copy-start.9
  213.2 0.7 copy-start.10
  213.3 214.3 %all-gather.17.cloned.1.call-start = ((), (), s32[]{:S(2)}) async-start(), calls=%async_computation.5 | async-start | bytes 7077888 | tf_op jit(solution)/shard_map/all_gather | solution.py:48
  214.0 54.6 %copy-start = (bf16[1,384,2,512]{3,1,0,2:T(8,128)(2,1)S(1)}, bf16[1,384,2,512]{3,1,0,2:T(8,128)(2,1)}, u32[]{:S(2)}) copy-start(bf16[1,384,2,512]{3,1,0,2:T(8,128)(2,1)} %all_to_all.30) | copy-start | bytes 2359300
  296.4 1.4 copy-start.4
  297.8 177.0 %all-gather.25.cloned.1.call-start = ((), (), s32[]{:S(2)}) async-start(), calls=%async_computation.9 | async-start | bytes 2621440 | tf_op jit(solution)/shard_map/all_gather | solution.py:37
  298.8 209.5 %all-gather.21.cloned.1.call-start = ((), (), s32[]{:S(2)}) async-start(), calls=%async_computation.7 | async-start | bytes 3538944 | tf_op jit(solution)/shard_map/all_gather | solution.py:61
  436.8 4.7 collective-permute-start.1
  442.7 69.9 %copy-start.1 = (bf16[768,512]{1,0:T(8,128)(2,1)S(1)}, bf16[768,512]{1,0:T(8,128)(2,1)}, u32[]{:S(2)}) copy-start(bf16[768,512]{1,0:T(8,128)(2,1)} %add_convert_fusion.1) | copy-start | bytes 2359300
Sparse Core Ops, SparseCore 0:
  13.9 118.0 all-gather.10
  133.9 44.7 all-gather.12
  180.3 48.0 all-gather.22
  230.1 34.1 all-gather.14
  265.7 115.3 all-gather.18
  382.8 44.7 all-gather.16
  429.1 45.6 all-gather.24
  476.7 31.5 all-gather.20
